TPU v7x, 32 devices: a whole 2x2x4 slice. The times are simulated.
32 devices in a mesh: rep: 2 (over x), fs: 8 (over z, y), tp: 2 (over core).
Axes of the slice: x: 2, y: 2, z: 4, core: 2. Of those that a mesh axis runs over, the one named last changes fastest.
Arguments:
- tokens: bfloat16 [6144, 2048], P(('rep', 'fs')), may hold values from -6 to 6
- first_gain: float32 [2048], replicated, may hold values from 0.1 to 1.9
- mixer_gate: bfloat16 [2048, 2048], P('fs', 'tp'), may hold values from -0.125 to 0.125
- mixer_value: bfloat16 [2048, 2048], P('fs', 'tp'), may hold values from -1 to 1
- value_gain: float32 [2048], replicated, may hold values from 0.1 to 1.9
- value_shift: float32 [2048], replicated, may hold values from -3 to 3
- spatial_weight: bfloat16 [16, 128, 128], replicated, may hold values from -0.75 to 0.75
- spatial_bias: float32 [16, 128], replicated, may hold values from 0.1 to 1.9
- mixer_out: bfloat16 [2048, 2048], P('tp', 'fs'), may hold values from -0.125 to 0.125
- second_gain: float32 [2048], replicated, may hold values from 0.1 to 1.9
- up_gate: bfloat16 [2048, 4096], P('fs', 'tp'), may hold values from -0.125 to 0.125
- up_value: bfloat16 [2048, 4096], P('fs', 'tp'), may hold values from -0.125 to 0.125
- taps_gate: float32 [3, 4096], replicated, may hold values from -3.5 to 3.5
- taps_value: float32 [3, 4096], replicated, may hold values from -3.5 to 3.5
- down_proj: bfloat16 [4096, 2048], P('tp', 'fs'), may hold values from -0.09375 to 0.09375
Outputs:
- layer_out: bfloat16 [6144, 2048], P(('rep', 'fs'))
All inputs are finite; a program needn't handle non-finite values.
Results may differ from a plain program's by a relative error of at most 0.015.
Values may be sent and summed in bfloat16 or wider, within the bound.
No kernel may reach another device: no remote copies, remote signals or barrier semaphores. Data moves between devices by JAX's collectives and lax.ppermute only.
A program may use at most 64 MiB of HBM per device.

v0:
```python
import jax
import jax.numpy as jnp
from jax import lax
from jax.sharding import PartitionSpec as P

D = 2048
GDIM = 128
BLK = 128
LEN = 128


def normalize(matrix, scale_gain):
    values = matrix.astype(jnp.float32)
    factor = lax.rsqrt(jnp.mean(values * values, axis=-1, keepdims=True) + 1e-06)
    return (values * factor * scale_gain).astype(jnp.bfloat16)


def causal_conv(values, tap_weights):
    by_sequence = values.reshape(-1, LEN, values.shape[-1])
    padded = jnp.pad(by_sequence, ((0, 0), (2, 0), (0, 0)))
    summed = (
        tap_weights[0] * padded[:, 0:LEN]
        + tap_weights[1] * padded[:, 1 : LEN + 1]
        + tap_weights[2] * padded[:, 2 : LEN + 2]
    )
    return summed.reshape(values.shape)


def local(
    tokens,
    first_gain,
    mixer_gate,
    mixer_value,
    value_gain,
    value_shift,
    spatial_weight,
    spatial_bias,
    mixer_out,
    second_gain,
    up_gate,
    up_value,
    taps_gate,
    taps_value,
    down_proj,
):
    tp_index = lax.axis_index("tp")
    first = normalize(tokens, first_gain)
    row_count = first.shape[0]
    local_cols = mixer_gate.shape[1]
    gate_acc = jnp.dot(
        first,
        lax.all_gather(mixer_gate, "fs", axis=0, tiled=True),
        preferred_element_type=jnp.float32,
    )
    value_acc = jnp.dot(
        first,
        lax.all_gather(mixer_value, "fs", axis=0, tiled=True),
        preferred_element_type=jnp.float32,
    )
    gate_act = jax.nn.gelu(gate_acc)
    value_act = jax.nn.gelu(value_acc)
    value_sum, value_squares = lax.psum(
        (jnp.sum(value_act, axis=1), jnp.sum(value_act * value_act, axis=1)), "tp"
    )
    row_mean = value_sum / D
    variance = value_squares / D - row_mean * row_mean
    col_gain = lax.dynamic_slice_in_dim(value_gain, tp_index * local_cols, local_cols)
    col_shift = lax.dynamic_slice_in_dim(value_shift, tp_index * local_cols, local_cols)
    centred = (
        (value_act - row_mean[:, None]) * lax.rsqrt(variance[:, None] + 1e-05) * col_gain
        + col_shift
    ).astype(jnp.bfloat16)
    local_groups = local_cols // GDIM
    local_weights = lax.dynamic_slice_in_dim(
        spatial_weight, tp_index * local_groups, local_groups, 0
    )
    biases = lax.dynamic_slice_in_dim(spatial_bias, tp_index * local_groups, local_groups, 0)
    masked = local_weights * jnp.tril(jnp.ones((BLK, BLK), jnp.bfloat16))
    blocks = centred.reshape(row_count // BLK, BLK, local_groups, GDIM)
    mixed_rows = (
        jnp.einsum("gts,bsgc->btgc", masked, blocks, preferred_element_type=jnp.float32)
        + biases.T[None, :, :, None]
    )
    gated_rows = (gate_act * mixed_rows.reshape(row_count, local_cols)).astype(jnp.bfloat16)
    whole_out = lax.all_gather(mixer_out, "fs", axis=1, tiled=True)
    row_share = row_count // lax.axis_size("tp")
    summed = lax.psum(
        jnp.dot(gated_rows, whole_out, preferred_element_type=jnp.float32).astype(jnp.bfloat16),
        "tp",
    ).astype(jnp.float32)
    residual = (tokens.astype(jnp.float32) + summed).astype(jnp.bfloat16)
    second = normalize(residual, second_gain)
    kept_rows = lax.dynamic_slice_in_dim(residual, tp_index * row_share, row_share, 0)
    hidden_cols = up_gate.shape[1]

    def add_rows(portion):
        return jnp.dot(second, portion, preferred_element_type=jnp.float32)

    gate_up = add_rows(lax.all_gather(up_gate, "fs", axis=0, tiled=True))
    value_up = add_rows(lax.all_gather(up_value, "fs", axis=0, tiled=True))
    gate_taps = lax.dynamic_slice_in_dim(taps_gate, tp_index * hidden_cols, hidden_cols, 1)
    value_taps = lax.dynamic_slice_in_dim(taps_value, tp_index * hidden_cols, hidden_cols, 1)
    hidden = (
        jax.nn.silu(causal_conv(gate_up, gate_taps)) * causal_conv(value_up, value_taps)
    ).astype(jnp.bfloat16)
    whole_down = lax.all_gather(down_proj, "fs", axis=1, tiled=True)
    ffn_total = lax.psum_scatter(
        jnp.dot(hidden, whole_down, preferred_element_type=jnp.float32).astype(jnp.bfloat16),
        "tp",
        scatter_dimension=0,
        tiled=True,
    ).astype(jnp.float32)
    final_rows = (kept_rows.astype(jnp.float32) + ffn_total).astype(jnp.bfloat16)
    return lax.all_gather(final_rows, "tp", axis=0, tiled=True)


def solution(mesh):
    in_specs = (
        P(("rep", "fs"), None),
        P(),
        P("fs", "tp"),
        P("fs", "tp"),
        P(),
        P(),
        P(),
        P(),
        P("tp", "fs"),
        P(),
        P("fs", "tp"),
        P("fs", "tp"),
        P(),
        P(),
        P("tp", "fs"),
    )
    out_specs = P(("rep", "fs"), None)
    return jax.shard_map(local, mesh=mesh, in_specs=in_specs, out_specs=out_specs, check_vma=False)
```

profile of v0, /device:TPU:0, one launch (start us, length us, event | category | flops | bytes accessed | tf_op | source)
XLA Modules:
  0.0 677.7 jit_solution(8803535783752608188)
XLA Ops:
  6.5 0.7 all-gather.10.cloned.1.call-update
  7.3 0.7 all-gather.12.cloned.1.call-update
  8.1 0.7 all-gather.8.cloned.1.call-update
  8.8 1.8 fusion.11
  10.7 74.3 %all-gather.10.cloned.1.call-done = bf16[2048,1024]{1,0:T(8,128)(2,1)} async-done(((bf16[256,1024]{1,0:T(8,128)(2,1)}), bf16[2048,1024]{1,0:T(8,128)(2,1)}) %all-gather.10.cloned.1.call-update) | async-done | bytes 4194320 | tf_op jit(solution)/shard_map/all_gather | solution.py:57
  85.0 4.5 fusion.66
  89.6 2.5 all-reduce.2
  92.6 0.5 copy-done.5
  93.1 0.4 bitcast_add_fusion
  93.5 1.6 copy.17
  95.2 65.1 %all-gather.12.cloned.1.call-done = bf16[1024,2048]{1,0:T(8,128)(2,1)} async-done(((bf16[1024,256]{1,0:T(8,128)(2,1)}), bf16[1024,2048]{1,0:T(8,128)(2,1)}) %all-gather.12.cloned.1.call-update) | async-done | bytes 4194320 | tf_op jit(solution)/shard_map/all_gather | solution.py:85
  160.3 73.1 %all-gather.8.cloned.1.call-done = bf16[2048,1024]{1,0:T(8,128)(2,1)} async-done(((bf16[256,1024]{1,0:T(8,128)(2,1)}), bf16[2048,1024]{1,0:T(8,128)(2,1)}) %all-gather.8.cloned.1.call-update) | async-done | bytes 4194320 | tf_op jit(solution)/shard_map/all_gather | solution.py:52
  233.4 9.0 %convolution_convert_fusion.1 = bf16[384,2048]{1,0:T(8,128)(2,1)} fusion(bf16[1024,2048]{1,0:T(8,128)(2,1)} %all-gather.12.cloned.1.call-done, f32[48,8,8,128]{3,2,1,0:T(8,128)} %bitcast.53, bf16[2048,1024]{1,0:T(8,128)(2,1)} %all-gather.8.cloned.1.call-done, bf16[384,2048]{1,0:T(8,128)(2,1)S(1)} %copy-done.2, f32[2048]{0:T(1024)S(1)} %copy-done.6, ...), kind=kOutput, calls=%fused_computation.32 | convolution fusion | flops 3229089792 | bytes 13116928 | tf_op jit(solution)/shard_map/dot_general | solution.py:88
  242.5 0.5 all-gather.14.cloned.1.call-update
  243.1 0.5 all-gather.16.cloned.1.call-update
  243.7 0.7 all-gather.18.cloned.1.call-update
  244.6 1.0 constant_dynamic-slice_fusion
  245.6 15.9 %all-reduce.5.cloned.1.call-done = bf16[384,2048]{1,0:T(8,128)(2,1)} async-done(((bf16[384,2048]{1,0:T(8,128)(2,1)}), bf16[384,2048]{1,0:T(8,128)(2,1)}) %all-reduce.5.cloned.1.call-update) | async-done | bytes 1572880 | tf_op jit(solution)/shard_map/psum | solution.py:87
  261.5 2.2 fusion.8
  263.7 125.5 %all-gather.14.cloned.1.call-done = bf16[2048,2048]{1,0:T(8,128)(2,1)} async-done(((bf16[256,2048]{1,0:T(8,128)(2,1)}), bf16[2048,2048]{1,0:T(8,128)(2,1)}) %all-gather.14.cloned.1.call-update) | async-done | bytes 8388624 | tf_op jit(solution)/shard_map/all_gather | solution.py:99
  389.2 5.9 fusion.54
  395.1 0.9 fusion.2
  396.1 117.8 %all-gather.16.cloned.1.call-done = bf16[2048,2048]{1,0:T(8,128)(2,1)} async-done(((bf16[256,2048]{1,0:T(8,128)(2,1)}), bf16[2048,2048]{1,0:T(8,128)(2,1)}) %all-gather.16.cloned.1.call-update) | async-done | bytes 8388624 | tf_op jit(solution)/shard_map/all_gather | solution.py:100
  513.8 6.4 fusion.52
  520.2 0.9 fusion.6
  521.2 2.2 fusion.15
  523.3 115.7 %all-gather.18.cloned.1.call-done = bf16[2048,2048]{1,0:T(8,128)(2,1)} async-done(((bf16[2048,256]{1,0:T(8,128)(2,1)}), bf16[2048,2048]{1,0:T(8,128)(2,1)}) %all-gather.18.cloned.1.call-update) | async-done | bytes 8388624 | tf_op jit(solution)/shard_map/all_gather | solution.py:106
  639.0 8.5 %convolution_convert_fusion = bf16[384,2048]{1,0:T(8,128)(2,1)} fusion(bf16[384,2048]{1,0:T(8,128)(2,1)} %fusion.15, bf16[2048,2048]{1,0:T(8,128)(2,1)} %all-gather.18.cloned.1.call-done), kind=kOutput, calls=%fused_computation.31 | convolution fusion | flops 3222011904 | bytes 11534336 | tf_op jit(solution)/shard_map/dot_general | solution.py:108
  647.6 7.3 %reduce-scatter.2.cloned.1.call-done = bf16[192,2048]{1,0:T(8,128)(2,1)} async-done(((bf16[384,2048]{1,0:T(8,128)(2,1)}), bf16[192,2048]{1,0:T(8,128)(2,1)}) %reduce-scatter.2.cloned.1.call-update) | async-done | bytes 786448 | tf_op jit(solution)/shard_map/reduce_scatter | solution.py:107
  654.9 2.3 add_convert_fusion
  657.2 11.2 %all-gather.20.cloned.1.call-done = bf16[384,2048]{1,0:T(8,128)(2,1)} async-done(((bf16[192,2048]{1,0:T(8,128)(2,1)}), bf16[384,2048]{1,0:T(8,128)(2,1)}) %all-gather.20.cloned.1.call-update) | async-done | bytes 1572880 | tf_op jit(solution)/shard_map/all_gather | solution.py:114
  668.5 2.7 copy.27
  (38 shorter events, 1.2 us)
Async XLA Ops:
  6.5 2.3 copy-start
  6.5 78.5 %copy-start.2 = (bf16[384,2048]{1,0:T(8,128)(2,1)S(1)}, bf16[384,2048]{1,0:T(8,128)(2,1)}, u32[]{:S(2)}) copy-start(bf16[384,2048]{1,0:T(8,128)(2,1)} %param.15) | copy-start | bytes 4718596
  6.5 78.5 %copy-start.6 = (f32[2048]{0:T(1024)S(1)}, f32[2048]{0:T(1024)}, u32[]{:S(2)}) copy-start(f32[2048]{0:T(1024)} %param.16) | copy-start | bytes 24580
  6.5 78.5 %all-gather.10.cloned.1.call-start = ((), (), s32[]{:S(2)}) async-start(), calls=%async_computation.2 | async-start | bytes 4718592 | tf_op jit(solution)/shard_map/all_gather | solution.py:57
  7.3 153.0 %all-gather.12.cloned.1.call-start = ((), (), s32[]{:S(2)}) async-start(), calls=%async_computation.3 | async-start | bytes 4718592 | tf_op jit(solution)/shard_map/all_gather | solution.py:85
  8.0 225.4 %all-gather.8.cloned.1.call-start = ((), (), s32[]{:S(2)}) async-start(), calls=%async_computation.1 | async-start | bytes 4718592 | tf_op jit(solution)/shard_map/all_gather | solution.py:52
  8.7 252.8 %all-reduce.5.cloned.1.call-start = ((), (), s32[]{:S(2)}) async-start(), calls=%async_computation.4 | async-start | bytes 3145728 | tf_op jit(solution)/shard_map/psum | solution.py:87
  10.6 81.4 %dynamic-slice-start = ((f32[2048]{0:T(1024)}, s32[]{:T(128)}), f32[1024]{0:T(1024)S(1)}, s32[]{:S(2)}) async-start(f32[2048]{0:T(1024)} %param.19, s32[]{:T(128)} %select_n.23), calls=%async_computation.10 | async-start | bytes 8704 | tf_op jit(solution)/shard_map/dynamic_slice | solution.py:67
  10.7 81.4 %dynamic-slice-start.1 = ((f32[2048]{0:T(1024)}, s32[]{:T(128)}), f32[1024]{0:T(1024)S(1)}, s32[]{:S(2)}) async-start(f32[2048]{0:T(1024)} %param.20, s32[]{:T(128)} %select_n.23), calls=%async_computation.11 | async-start | bytes 8704 | tf_op jit(solution)/shard_map/dynamic_slice | solution.py:68
  92.0 1.1 copy-start.5
  242.5 146.7 %all-gather.14.cloned.1.call-start = ((), (), s32[]{:S(2)}) async-start(), calls=%async_computation.5 | async-start | bytes 9437184 | tf_op jit(solution)/shard_map/all_gather | solution.py:99
  243.0 270.8 %all-gather.16.cloned.1.call-start = ((), (), s32[]{:S(2)}) async-start(), calls=%async_computation.6 | async-start | bytes 9437184 | tf_op jit(solution)/shard_map/all_gather | solution.py:100
  243.6 145.6 %copy-start.7 = (f32[2048]{0:T(1024)S(1)}, f32[2048]{0:T(1024)}, u32[]{:S(2)}) copy-start(f32[2048]{0:T(1024)} %param.24) | copy-start | bytes 24580
  243.6 395.4 %all-gather.18.cloned.1.call-start = ((), (), s32[]{:S(2)}) async-start(), calls=%async_computation.7 | async-start | bytes 9437184 | tf_op jit(solution)/shard_map/all_gather | solution.py:106
  244.4 410.5 %reduce-scatter.2.cloned.1.call-start = ((), (), s32[]{:S(2)}) async-start(), calls=%async_computation.8 | async-start | bytes 2359296 | tf_op jit(solution)/shard_map/reduce_scatter | solution.py:107
  263.7 131.5 %copy-start.3 = (bf16[384,2048]{1,0:T(8,128)(2,1)}, bf16[384,2048]{1,0:T(8,128)(2,1)S(1)}, u32[]{:S(2)}) copy-start(bf16[384,2048]{1,0:T(8,128)(2,1)S(1)} %get-tuple-element.10) | copy-start | bytes 4718596
  523.3 131.6 %copy-start.4 = (bf16[384,2048]{1,0:T(8,128)(2,1)S(1)}, bf16[384,2048]{1,0:T(8,128)(2,1)}, u32[]{:S(2)}) copy-start(bf16[384,2048]{1,0:T(8,128)(2,1)} %copy-done.3) | copy-start | bytes 4718596
  647.5 20.9 %all-gather.20.cloned.1.call-start = ((), (), s32[]{:S(2)}) async-start(), calls=%async_computation.9 | async-start | bytes 2359296 | tf_op jit(solution)/shard_map/all_gather | solution.py:114
  647.6 23.6 %copy-start.1 = (f32[16,128]{1,0:T(8,128)S(1)}, f32[16,128]{1,0:T(8,128)}, u32[]{:S(2)}) copy-start(f32[16,128]{1,0:T(8,128)} %param.22) | copy-start | bytes 24580
Sparse Core Ops, SparseCore 0:
  9.5 75.5 all-gather.9
  87.1 73.1 all-gather.11
  162.4 70.9 all-gather.7
  242.6 18.8 all-reduce.4
  263.5 125.6 all-gather.13
  391.2 122.6 all-gather.15
  515.9 123.1 all-gather.17
  647.7 7.2 reduce-scatter.1
  657.3 11.0 all-gather.19
where the time goes:
time: 678 us
  waiting for transfers between devices  610 us (90%)
  matrix products  34.8 us (5%)
  between operations  13.4 us (2%)
  other arithmetic  10.6 us (2%)
    all_gather x1, waiting for transfers between devices, local(): gate_up = add_rows(lax.all_gather(up_gate, 'fs', axis=0, tiled=True))  125 us
    all_gather x1, waiting for transfers between devices, local(): value_up = add_rows(lax.all_gather(up_value, 'fs', axis=0, tiled=True))  118 us
    all_gather x1, waiting for transfers between devices, local(): whole_down = lax.all_gather(down_proj, 'fs', axis=1, tiled=True)  116 us
    all_gather x1, waiting for transfers between devices, local(): lax.all_gather(mixer_value, 'fs', axis=0, tiled=True)  74.3 us
    all_gather x1, waiting for transfers between devices, local(): lax.all_gather(mixer_gate, 'fs', axis=0, tiled=True)  73.1 us
    all_gather x1, waiting for transfers between devices, local(): whole_out = lax.all_gather(mixer_out, 'fs', axis=1, tiled=True)  65.1 us
    psum x1, waiting for transfers between devices, local(): lax.psum(jnp.dot(gated_rows, whole_out, preferred_element_type=jnp.float3...  15.9 us
  transfers between devices with their start and end apart: 9, of which 9 were waited for; matrix products, arithmetic and copies ran while one was open for 4% of the time, Pallas kernels for 0%

commit v1 on v0

--- a/solution.py
+++ b/solution.py
@@ -82,7 +82,12 @@
         + biases.T[None, :, :, None]
     )
     gated_rows = (gate_act * mixed_rows.reshape(row_count, local_cols)).astype(jnp.bfloat16)
-    whole_out = lax.all_gather(mixer_out, "fs", axis=1, tiled=True)
+    ring = [mixer_out]
+    for hop in range(7):
+        ring.append(lax.ppermute(ring[-1], "fs", [(dev, (dev + 1) % 8) for dev in range(8)]))
+    whole_out = jnp.roll(
+        jnp.concatenate(ring[::-1], axis=1), (lax.axis_index("fs") + 1) * ring[0].shape[1], axis=1
+    )
     row_share = row_count // lax.axis_size("tp")
     summed = lax.psum(
         jnp.dot(gated_rows, whole_out, preferred_element_type=jnp.float32).astype(jnp.bfloat16),

time: 678 us -> 652 us (0.962)
  waiting for transfers between devices: 610 us -> 565 us
  local copies, waits for them, and re-layouts: 6.08 us -> 20.2 us
    ppermute x0 -> x7, waiting for transfers between devices: none -> 153 us  [local(): lax.ppermute(ring[-1], 'fs', [(dev, (dev + 1) % 8) for dev in range(8)])]
    all_gather x1, waiting for transfers between devices: 74.3 us -> 0.01 us  [local(): lax.all_gather(mixer_value, 'fs', axis=0, tiled=True)]
    all_gather x1 -> x0, waiting for transfers between devices: 65.1 us -> none  [local(): whole_out = lax.all_gather(mixer_out, 'fs', axis=1, tiled=True)]
    all_gather x1, waiting for transfers between devices: 73.1 us -> 15.2 us  [local(): lax.all_gather(mixer_gate, 'fs', axis=0, tiled=True)]
    unnamed x18 -> x43, local copies, waits for them, and re-layouts: 3.44 us -> 16.7 us
  transfers between devices with their start and end apart: 9 -> 15, of which waited for: 9 -> 14; matrix products, arithmetic and copies ran while one was open for 4% -> 7% of each run, Pallas kernels for 0% -> 0%
where the time goes in v1:
time: 652 us; the launch traced here: 651 us
  waiting for transfers between devices  565 us (87%)
  matrix products  34.8 us (5%)
  local copies, waits for them, and re-layouts  20.2 us (3%)
  between operations  13.7 us (2%)
  other arithmetic  10.7 us (2%)
    ppermute x7, waiting for transfers between devices, local(): lax.ppermute(ring[-1], 'fs', [(dev, (dev + 1) % 8) for dev in range(8)])  153 us
    all_gather x1, waiting for transfers between devices, local(): gate_up = add_rows(lax.all_gather(up_gate, 'fs', axis=0, tiled=True))  125 us
    all_gather x1, waiting for transfers between devices, local(): value_up = add_rows(lax.all_gather(up_value, 'fs', axis=0, tiled=True))  118 us
    all_gather x1, waiting for transfers between devices, local(): whole_down = lax.all_gather(down_proj, 'fs', axis=1, tiled=True)  116 us
    unnamed x43, local copies, waits for them, and re-layouts  16.7 us
    psum x1, waiting for transfers between devices, local(): lax.psum(jnp.dot(gated_rows, whole_out, preferred_element_type=jnp.float3...  16.1 us
    all_gather x1, waiting for transfers between devices, local(): lax.all_gather(mixer_gate, 'fs', axis=0, tiled=True)  15.2 us
  transfers between devices with their start and end apart: 15, of which 14 were waited for; matrix products, arithmetic and copies ran while one was open for 7% of the time, Pallas kernels for 0%

profile of v1, /device:TPU:0, one launch (start us, length us, event | category | flops | bytes accessed | tf_op | source)
XLA Modules:
  0.0 651.3 jit_solution(12675379626138669287)
XLA Ops:
  8.1 3.0 collective-permute-start
  11.1 15.7 %collective-permute-done = bf16[1024,256]{1,0:T(8,128)(2,1)S(1)} collective-permute-done((bf16[1024,256]{1,0:T(8,128)(2,1)}, bf16[1024,256]{1,0:T(8,128)(2,1)S(1)}, u32[]{:S(2)}, u32[]{:S(2)}) %collective-permute-start) | collective-permute-done | bytes 524320 | tf_op jit(solution)/shard_map/ppermute | solution.py:87
  26.8 1.0 collective-permute-start.1
  27.8 26.6 %collective-permute-done.1 = bf16[1024,256]{1,0:T(8,128)(2,1)S(1)} collective-permute-done((bf16[1024,256]{1,0:T(8,128)(2,1)S(1)}, bf16[1024,256]{1,0:T(8,128)(2,1)S(1)}, u32[]{:S(2)}, u32[]{:S(2)}) %collective-permute-start.1) | collective-permute-done | bytes 524320 | tf_op jit(solution)/shard_map/ppermute | solution.py:87
  54.4 25.6 %collective-permute-done.2 = bf16[1024,256]{1,0:T(8,128)(2,1)S(1)} collective-permute-done((bf16[1024,256]{1,0:T(8,128)(2,1)S(1)}, bf16[1024,256]{1,0:T(8,128)(2,1)S(1)}, u32[]{:S(2)}, u32[]{:S(2)}) %collective-permute-start.2) | collective-permute-done | bytes 524320 | tf_op jit(solution)/shard_map/ppermute | solution.py:87
  80.0 26.9 %collective-permute-done.3 = bf16[1024,256]{1,0:T(8,128)(2,1)S(1)} collective-permute-done((bf16[1024,256]{1,0:T(8,128)(2,1)S(1)}, bf16[1024,256]{1,0:T(8,128)(2,1)S(1)}, u32[]{:S(2)}, u32[]{:S(2)}) %collective-permute-start.3) | collective-permute-done | bytes 524320 | tf_op jit(solution)/shard_map/ppermute | solution.py:87
  106.9 18.7 %collective-permute-done.4 = bf16[1024,256]{1,0:T(8,128)(2,1)S(1)} collective-permute-done((bf16[1024,256]{1,0:T(8,128)(2,1)S(1)}, bf16[1024,256]{1,0:T(8,128)(2,1)S(1)}, u32[]{:S(2)}, u32[]{:S(2)}) %collective-permute-start.4) | collective-permute-done | bytes 524320 | tf_op jit(solution)/shard_map/ppermute | solution.py:87
  125.6 22.1 %collective-permute-done.5 = bf16[1024,256]{1,0:T(8,128)(2,1)S(1)} collective-permute-done((bf16[1024,256]{1,0:T(8,128)(2,1)S(1)}, bf16[1024,256]{1,0:T(8,128)(2,1)S(1)}, u32[]{:S(2)}, u32[]{:S(2)}) %collective-permute-start.5) | collective-permute-done | bytes 524320 | tf_op jit(solution)/shard_map/ppermute | solution.py:87
  147.7 1.8 fusion.13
  149.5 17.8 %collective-permute-done.6 = bf16[1024,256]{1,0:T(8,128)(2,1)S(1)} collective-permute-done((bf16[1024,256]{1,0:T(8,128)(2,1)S(1)}, bf16[1024,256]{1,0:T(8,128)(2,1)S(1)}, u32[]{:S(2)}, u32[]{:S(2)}) %collective-permute-start.6) | collective-permute-done | bytes 524320 | tf_op jit(solution)/shard_map/ppermute | solution.py:87
  176.1 0.9 constant_dynamic-update-slice_fusion.5
  181.5 4.6 fusion.72
  186.1 2.5 all-reduce.2
  190.0 1.6 copy.17
  191.7 15.2 %all-gather.7.cloned.1.call-done = bf16[2048,1024]{1,0:T(8,128)(2,1)} async-done(((bf16[256,1024]{1,0:T(8,128)(2,1)}), bf16[2048,1024]{1,0:T(8,128)(2,1)}) %all-gather.7.cloned.1.call-update) | async-done | bytes 4194320 | tf_op jit(solution)/shard_map/all_gather | solution.py:52
  206.9 9.0 %fusion.21 = bf16[384,2048]{1,0:T(8,128)(2,1)} fusion(bf16[1024,4096]{1,0:T(8,128)(2,1)} %constant_dynamic-update-slice_fusion, s32[]{:T(128)S(6)} %select_n.40, f32[48,8,8,128]{3,2,1,0:T(8,128)} %bitcast.52, bf16[2048,1024]{1,0:T(8,128)(2,1)} %all-gather.7.cloned.1.call-done, bf16[384,2048]{1,0:T(8,128)(2,1)S(1)} %copy-done.2, f32[2048]{0:T(1024)S(1)} %copy-done.11, ...), kind=kOutput, calls=%fused_computation.34 | convolution fusion | flops 3229089792 | bytes 13116932 | tf_op jit(solution)/shard_map/dot_general | solution.py:93
  217.9 1.0 constant_dynamic-slice_fusion
  218.9 16.1 %all-reduce.5.cloned.1.call-done = bf16[384,2048]{1,0:T(8,128)(2,1)} async-done(((bf16[384,2048]{1,0:T(8,128)(2,1)}), bf16[384,2048]{1,0:T(8,128)(2,1)}) %all-reduce.5.cloned.1.call-update) | async-done | bytes 1572880 | tf_op jit(solution)/shard_map/psum | solution.py:92
  235.0 2.2 fusion.10
  237.2 125.5 %all-gather.11.cloned.1.call-done = bf16[2048,2048]{1,0:T(8,128)(2,1)} async-done(((bf16[256,2048]{1,0:T(8,128)(2,1)}), bf16[2048,2048]{1,0:T(8,128)(2,1)}) %all-gather.11.cloned.1.call-update) | async-done | bytes 8388624 | tf_op jit(solution)/shard_map/all_gather | solution.py:104
  362.6 6.0 fusion.55
  368.6 0.9 fusion.4
  369.5 117.8 %all-gather.13.cloned.1.call-done = bf16[2048,2048]{1,0:T(8,128)(2,1)} async-done(((bf16[256,2048]{1,0:T(8,128)(2,1)}), bf16[2048,2048]{1,0:T(8,128)(2,1)}) %all-gather.13.cloned.1.call-update) | async-done | bytes 8388624 | tf_op jit(solution)/shard_map/all_gather | solution.py:105
  487.3 6.4 fusion.53
  493.7 0.9 fusion.8
  494.6 2.2 fusion.17
  496.8 115.6 %all-gather.15.cloned.1.call-done = bf16[2048,2048]{1,0:T(8,128)(2,1)} async-done(((bf16[2048,256]{1,0:T(8,128)(2,1)}), bf16[2048,2048]{1,0:T(8,128)(2,1)}) %all-gather.15.cloned.1.call-update) | async-done | bytes 8388624 | tf_op jit(solution)/shard_map/all_gather | solution.py:111
  612.4 8.5 %convolution_convert_fusion = bf16[384,2048]{1,0:T(8,128)(2,1)} fusion(bf16[384,2048]{1,0:T(8,128)(2,1)} %fusion.17, bf16[2048,2048]{1,0:T(8,128)(2,1)} %all-gather.15.cloned.1.call-done), kind=kOutput, calls=%fused_computation.33 | convolution fusion | flops 3222011904 | bytes 11534336 | tf_op jit(solution)/shard_map/dot_general | solution.py:113
  620.9 7.3 %reduce-scatter.2.cloned.1.call-done = bf16[192,2048]{1,0:T(8,128)(2,1)} async-done(((bf16[384,2048]{1,0:T(8,128)(2,1)}), bf16[192,2048]{1,0:T(8,128)(2,1)}) %reduce-scatter.2.cloned.1.call-update) | async-done | bytes 786448 | tf_op jit(solution)/shard_map/reduce_scatter | solution.py:112
  628.2 2.3 add_convert_fusion
  630.5 11.2 %all-gather.17.cloned.1.call-done = bf16[384,2048]{1,0:T(8,128)(2,1)} async-done(((bf16[192,2048]{1,0:T(8,128)(2,1)}), bf16[384,2048]{1,0:T(8,128)(2,1)}) %all-gather.17.cloned.1.call-update) | async-done | bytes 1572880 | tf_op jit(solution)/shard_map/all_gather | solution.py:119
  641.8 2.7 copy.42
  (75 shorter events, 18.2 us)
Async XLA Ops:
  6.5 141.2 %copy-start = (f32[16,128]{1,0:T(8,128)S(1)}, f32[16,128]{1,0:T(8,128)}, u32[]{:S(2)}) copy-start(f32[16,128]{1,0:T(8,128)} %param.22) | copy-start | bytes 24580
  6.5 175.0 %all-gather.9.cloned.1.call-start = ((), (), s32[]{:S(2)}) async-start(), calls=%async_computation.2 | async-start | bytes 4718592 | tf_op jit(solution)/shard_map/all_gather | solution.py:57
  7.3 199.6 %all-gather.7.cloned.1.call-start = ((), (), s32[]{:S(2)}) async-start(), calls=%async_computation.1 | async-start | bytes 4718592 | tf_op jit(solution)/shard_map/all_gather | solution.py:52
  8.0 227.0 %all-reduce.5.cloned.1.call-start = ((), (), s32[]{:S(2)}) async-start(), calls=%async_computation.3 | async-start | bytes 3145728 | tf_op jit(solution)/shard_map/psum | solution.py:92
  8.1 18.8 %collective-permute-start = (bf16[1024,256]{1,0:T(8,128)(2,1)}, bf16[1024,256]{1,0:T(8,128)(2,1)S(1)}, u32[]{:S(2)}, u32[]{:S(2)}) collective-permute-start(bf16[1024,256]{1,0:T(8,128)(2,1)} %param.23), channel_id=1, source_target_pairs={{0,2},{2,4},{4,6},{6,8},{8,10},{10,12},{12,14},{14,0},{1,3},{3,5},... | collective-permute-start | bytes 1572872 | tf_op jit(solution)/shard_map/ppermute | solution.py:87
  26.8 27.6 %collective-permute-start.1 = (bf16[1024,256]{1,0:T(8,128)(2,1)S(1)}, bf16[1024,256]{1,0:T(8,128)(2,1)S(1)}, u32[]{:S(2)}, u32[]{:S(2)}) collective-permute-start(bf16[1024,256]{1,0:T(8,128)(2,1)S(1)} %collective-permute-done), channel_id=1, source_target_pairs={{0,2},{2,4},{4,6},{6,8},{8,10},{10,12},{12,14},{14,0},{1,3},{3,5},... | collective-permute-start | bytes 1572872 | tf_op jit(solution)/shard_map/ppermute | solution.py:87
  54.4 25.6 %collective-permute-start.2 = (bf16[1024,256]{1,0:T(8,128)(2,1)S(1)}, bf16[1024,256]{1,0:T(8,128)(2,1)S(1)}, u32[]{:S(2)}, u32[]{:S(2)}) collective-permute-start(bf16[1024,256]{1,0:T(8,128)(2,1)S(1)} %collective-permute-done.1), channel_id=1, source_target_pairs={{0,2},{2,4},{4,6},{6,8},{8,10},{10,12},{12,14},{14,0},{1,3},{3,5},... | collective-permute-start | bytes 1572872 | tf_op jit(solution)/shard_map/ppermute | solution.py:87
  80.0 26.9 %collective-permute-start.3 = (bf16[1024,256]{1,0:T(8,128)(2,1)S(1)}, bf16[1024,256]{1,0:T(8,128)(2,1)S(1)}, u32[]{:S(2)}, u32[]{:S(2)}) collective-permute-start(bf16[1024,256]{1,0:T(8,128)(2,1)S(1)} %collective-permute-done.2), channel_id=1, source_target_pairs={{0,2},{2,4},{4,6},{6,8},{8,10},{10,12},{12,14},{14,0},{1,3},{3,5},... | collective-permute-start | bytes 1572872 | tf_op jit(solution)/shard_map/ppermute | solution.py:87
  106.9 64.8 %copy-start.6 = (bf16[1024,256]{1,0:T(8,128)(2,1)}, bf16[1024,256]{1,0:T(8,128)(2,1)S(1)}, u32[]{:S(2)}) copy-start(bf16[1024,256]{1,0:T(8,128)(2,1)S(1)} %collective-permute-done.3) | copy-start | bytes 1572868
  106.9 18.7 %collective-permute-start.4 = (bf16[1024,256]{1,0:T(8,128)(2,1)S(1)}, bf16[1024,256]{1,0:T(8,128)(2,1)S(1)}, u32[]{:S(2)}, u32[]{:S(2)}) collective-permute-start(bf16[1024,256]{1,0:T(8,128)(2,1)S(1)} %collective-permute-done.3), channel_id=1, source_target_pairs={{0,2},{2,4},{4,6},{6,8},{8,10},{10,12},{12,14},{14,0},{1,3},{3,5},... | collective-permute-start | bytes 1572872 | tf_op jit(solution)/shard_map/ppermute | solution.py:87
  125.6 46.1 %copy-start.8 = (bf16[1024,256]{1,0:T(8,128)(2,1)}, bf16[1024,256]{1,0:T(8,128)(2,1)S(1)}, u32[]{:S(2)}) copy-start(bf16[1024,256]{1,0:T(8,128)(2,1)S(1)} %collective-permute-done.4) | copy-start | bytes 1572868
  125.6 22.1 %collective-permute-start.5 = (bf16[1024,256]{1,0:T(8,128)(2,1)S(1)}, bf16[1024,256]{1,0:T(8,128)(2,1)S(1)}, u32[]{:S(2)}, u32[]{:S(2)}) collective-permute-start(bf16[1024,256]{1,0:T(8,128)(2,1)S(1)} %collective-permute-done.4), channel_id=1, source_target_pairs={{0,2},{2,4},{4,6},{6,8},{8,10},{10,12},{12,14},{14,0},{1,3},{3,5},... | collective-permute-start | bytes 1572872 | tf_op jit(solution)/shard_map/ppermute | solution.py:87
  147.7 19.6 %collective-permute-start.6 = (bf16[1024,256]{1,0:T(8,128)(2,1)S(1)}, bf16[1024,256]{1,0:T(8,128)(2,1)S(1)}, u32[]{:S(2)}, u32[]{:S(2)}) collective-permute-start(bf16[1024,256]{1,0:T(8,128)(2,1)S(1)} %collective-permute-done.5), channel_id=1, source_target_pairs={{0,2},{2,4},{4,6},{6,8},{8,10},{10,12},{12,14},{14,0},{1,3},{3,5},... | collective-permute-start | bytes 1572872 | tf_op jit(solution)/shard_map/ppermute | solution.py:87
  168.2 5.3 copy-start.5
  172.6 3.5 copy-start.9
  172.6 4.4 copy-start.7
  176.1 5.4 copy-start.2
  176.1 5.4 copy-start.11
  181.5 7.1 %dynamic-slice-start = ((f32[2048]{0:T(1024)}, s32[]{:T(128)}), f32[1024]{0:T(1024)S(1)}, s32[]{:S(2)}) async-start(f32[2048]{0:T(1024)} %param.19, s32[]{:T(128)} %select_n.36), calls=%async_computation.9 | async-start | bytes 8704 | tf_op jit(solution)/shard_map/dynamic_slice | solution.py:67
  181.5 7.1 %dynamic-slice-start.1 = ((f32[2048]{0:T(1024)}, s32[]{:T(128)}), f32[1024]{0:T(1024)S(1)}, s32[]{:S(2)}) async-start(f32[2048]{0:T(1024)} %param.20, s32[]{:T(128)} %select_n.36), calls=%async_computation.10 | async-start | bytes 8704 | tf_op jit(solution)/shard_map/dynamic_slice | solution.py:68
  188.6 1.0 copy-start.10
  215.9 146.7 %all-gather.11.cloned.1.call-start = ((), (), s32[]{:S(2)}) async-start(), calls=%async_computation.4 | async-start | bytes 9437184 | tf_op jit(solution)/shard_map/all_gather | solution.py:104
  216.5 270.8 %all-gather.13.cloned.1.call-start = ((), (), s32[]{:S(2)}) async-start(), calls=%async_computation.5 | async-start | bytes 9437184 | tf_op jit(solution)/shard_map/all_gather | solution.py:105
  217.1 145.6 %copy-start.12 = (f32[2048]{0:T(1024)S(1)}, f32[2048]{0:T(1024)}, u32[]{:S(2)}) copy-start(f32[2048]{0:T(1024)} %param.24) | copy-start | bytes 24580
  217.1 395.3 %all-gather.15.cloned.1.call-start = ((), (), s32[]{:S(2)}) async-start(), calls=%async_computation.6 | async-start | bytes 9437184 | tf_op jit(solution)/shard_map/all_gather | solution.py:111
  217.6 410.6 %reduce-scatter.2.cloned.1.call-start = ((), (), s32[]{:S(2)}) async-start(), calls=%async_computation.7 | async-start | bytes 2359296 | tf_op jit(solution)/shard_map/reduce_scatter | solution.py:112
  237.1 131.5 %copy-start.3 = (bf16[384,2048]{1,0:T(8,128)(2,1)}, bf16[384,2048]{1,0:T(8,128)(2,1)S(1)}, u32[]{:S(2)}) copy-start(bf16[384,2048]{1,0:T(8,128)(2,1)S(1)} %get-tuple-element.10) | copy-start | bytes 4718596
  496.8 131.4 %copy-start.4 = (bf16[384,2048]{1,0:T(8,128)(2,1)S(1)}, bf16[384,2048]{1,0:T(8,128)(2,1)}, u32[]{:S(2)}) copy-start(bf16[384,2048]{1,0:T(8,128)(2,1)} %copy-done.3) | copy-start | bytes 4718596
  620.8 20.9 %all-gather.17.cloned.1.call-start = ((), (), s32[]{:S(2)}) async-start(), calls=%async_computation.8 | async-start | bytes 2359296 | tf_op jit(solution)/shard_map/all_gather | solution.py:119
  620.9 23.6 %copy-start.1 = (f32[16,128]{1,0:T(8,128)S(1)}, f32[16,128]{1,0:T(8,128)}, u32[]{:S(2)}) copy-start(f32[16,128]{1,0:T(8,128)} %param.22) | copy-start | bytes 24580
Sparse Core Ops, SparseCore 0:
  9.5 104.3 all-gather.8
  116.0 90.8 all-gather.6
  216.0 18.9 all-reduce.4
  236.9 125.6 all-gather.10
  364.6 122.6 all-gather.12
  489.2 123.1 all-gather.14
  621.0 7.2 reduce-scatter.1
  630.6 11.0 all-gather.16
